TPU v7x, 32 devices: a whole 2x2x4 slice. The times are simulated.
32 devices in a mesh: grp: 2 (over y), fs: 4 (over z), tp: 4 (over x, core).
Axes of the slice: x: 2, y: 2, z: 4, core: 2. Of those that a mesh axis runs over, the one named last changes fastest.
Arguments:
- tokens: bfloat16 [2048, 3072], P(('grp', 'tp')), parts along dimension 0, may hold values from -6 to 6
- up_master: float32 [3072, 12288], P('fs', 'tp'), may hold values from -0.109375 to 0.109375
- down_master: float32 [12288, 3072], P('fs', 'tp'), may hold values from -0.0546875 to 0.0546875
- norm_gain: float32 [3072], P('fs'), may hold values from 0.1 to 1.9
Outputs:
- prompt_out: bfloat16 [2048, 3072], P(('grp', 'tp'), 'fs'), parts along dimension 0
- sampled_up: bfloat16 [6144, 12288], P('grp', 'fs'), parts along dimension 0
- sampled_down: bfloat16 [24576, 3072], P(('grp', 'fs')), parts along dimension 0
There are 2 independent parts, one for each index of `grp`. A program takes and returns all parts, laid end to end along the dimension named above; an argument that names none is the same for every part. Nothing has to cross between parts.
All inputs are finite; a program needn't handle non-finite values.
Results may differ from a plain program's by a relative error of at most 0.0074.
Values may be sent and summed in bfloat16 or wider, within the bound.
A program may use at most 192 MiB of HBM per device.

v0:
```python
import jax
import jax.numpy as jnp
from jax import lax
from jax.sharding import PartitionSpec as P


def normalize(tokens):
    values = tokens.astype(jnp.float32)
    center = jnp.mean(values, axis=-1, keepdims=True)
    spread = jnp.mean(jnp.square(values - center), axis=-1, keepdims=True)
    return ((values - center) * lax.rsqrt(spread + 1e-05)).astype(jnp.bfloat16)


def shards(tokens, up_master, down_master, norm_gain):
    up_cast = (norm_gain[:, None] * up_master).astype(jnp.bfloat16)
    down_cast = down_master.astype(jnp.bfloat16)
    quarter = lax.all_to_all(up_cast, "tp", split_axis=0, concat_axis=1, tiled=True)
    moved = lax.all_to_all(quarter, "fs", split_axis=1, concat_axis=0, tiled=True)
    part_rows = quarter.shape[0]
    stacked = moved.reshape(moved.shape[0] // part_rows, part_rows, moved.shape[1])
    joined, sampled_down = (
        lax.all_gather(stacked, "tp", axis=1, tiled=True),
        lax.all_gather(down_cast, "tp", axis=1, tiled=True),
    )
    sampled_up = joined.reshape(joined.shape[0] * joined.shape[1], joined.shape[2])
    normalized = normalize(tokens)
    before = jnp.dot(normalized, sampled_up, preferred_element_type=jnp.float32)
    hidden = jnp.square(jax.nn.relu(before)).astype(jnp.bfloat16)
    terms = jnp.dot(hidden, sampled_down, preferred_element_type=jnp.float32)
    summed = lax.psum_scatter(terms, "fs", scatter_dimension=1, tiled=True)
    return (summed.astype(jnp.bfloat16), sampled_up, sampled_down)


def solution(mesh):
    return jax.shard_map(
        shards,
        mesh=mesh,
        in_specs=(P(("grp", "tp"), None), P("fs", "tp"), P("fs", "tp"), P("fs")),
        out_specs=(P(("grp", "tp"), "fs"), P("grp", "fs"), P(("grp", "fs"), None)),
        check_vma=False,
    )
```

profile of v0, /device:TPU:0, one launch (start us, length us, event | category | flops | bytes accessed | tf_op | source)
XLA Modules:
  0.0 525.0 jit_solution(6429137152449388254)
XLA Ops:
  7.2 0.0 all-gather.3.cloned.1.call-start
  7.2 5.1 multiply_convert_fusion
  12.3 57.8 %all_to_all.29 = bf16[4,192,3072]{2,1,0:T(8,128)(2,1)S(1)} all-to-all(bf16[4,192,3072]{2,1,0:T(8,128)(2,1)S(1)} %bitcast.13), channel_id=1, replica_groups=mesh['grp'=2,'fs'=4,'tp'=4] {'tp'}, dimensions={0} | all-to-all | bytes 9437184 | tf_op jit(solution)/shard_map/all_to_all | solution.py:17
  70.1 108.8 %all_to_all.30 = bf16[192,4,3072]{2,0,1:T(8,128)(2,1)} all-to-all(bf16[192,4,3072]{2,0,1:T(8,128)(2,1)S(1)} %bitcast.12), channel_id=1, replica_groups=mesh['grp'=2,'fs'=4,'tp'=4] {'fs'}, dimensions={1} | all-to-all | bytes 9437184 | tf_op jit(solution)/shard_map/all_to_all | solution.py:18
  178.9 0.0 all-gather.3.cloned.1.call-update
  178.9 0.0 all-gather.5.cloned.1.call-start
  179.0 6.7 %convert_element_type.22 = bf16[3072,768]{1,0:T(8,128)(2,1)} convert(f32[3072,768]{1,0:T(8,128)} %param.6) | non-fusion elementwise | flops 2359296 | bytes 14155776 | tf_op jit(solution)/shard_map/convert_element_type | solution.py:16
  185.7 0.0 all-gather.5.cloned.1.call-update
  185.7 0.0 reduce-scatter.2.cloned.1.call-start
  185.8 1.7 copy-done
  187.5 0.3 convert_reduce_fusion
  187.8 0.6 fusion.4
  188.4 108.7 %all-gather.3.cloned.1.call-done = bf16[4,768,3072]{2,1,0:T(8,128)(2,1)} async-done(((bf16[4,192,3072]{2,1,0:T(8,128)(2,1)}), bf16[4,768,3072]{2,1,0:T(8,128)(2,1)}) %all-gather.3.cloned.1.call-update) | async-done | bytes 18874384 | tf_op jit(solution)/shard_map/all_gather | solution.py:22
  297.0 9.4 %fusion.1 = bf16[256,3072]{1,0:T(8,128)(2,1)S(1)} fusion(bf16[3072,3072]{1,0:T(8,128)(2,1)} %bitcast.7, bf16[256,3072]{1,0:T(8,128)(2,1)S(1)} %copy-done, f32[256]{0:T(256)S(1)} %add_rsqrt_fusion, f32[256]{0:T(256)S(1)} %broadcast_multiply_fusion), kind=kOutput, calls=%fused_computation.5 | convolution fusion | flops 4837343232 | bytes 22022144 | tf_op jit(solution)/shard_map/dot_general | solution.py:27
  306.5 112.7 %all-gather.5.cloned.1.call-done = bf16[3072,3072]{1,0:T(8,128)(2,1)} async-done(((bf16[3072,768]{1,0:T(8,128)(2,1)}), bf16[3072,3072]{1,0:T(8,128)(2,1)}) %all-gather.5.cloned.1.call-update) | async-done | bytes 18874384 | tf_op jit(solution)/shard_map/all_gather | solution.py:23
  419.2 10.7 %fusion.9 = f32[256,3072]{1,0:T(8,128)} fusion(bf16[256,3072]{1,0:T(8,128)(2,1)S(1)} %fusion.1, bf16[3072,3072]{1,0:T(8,128)(2,1)} %all-gather.5.cloned.1.call-done), kind=kOutput, calls=%fused_computation.14 | convolution fusion | flops 4831838208 | bytes 23592960 | tf_op jit(solution)/shard_map/dot_general | solution.py:29
  429.9 0.0 reduce-scatter.2.cloned.1.call-update
  429.9 60.6 %reduce-scatter.2.cloned.1.call-done = f32[256,768]{1,0:T(8,128)} async-done(((f32[256,3072]{1,0:T(8,128)}), f32[256,768]{1,0:T(8,128)}) %reduce-scatter.2.cloned.1.call-update) | async-done | bytes 786448 | tf_op jit(solution)/shard_map/reduce_scatter | solution.py:30
  490.4 2.1 convert_element_type.23
  492.5 19.1 %copy.9 = bf16[3072,3072]{1,0:T(8,128)(2,1)} copy(bf16[3072,3072]{1,0:T(8,128)(2,1)} %bitcast.8) | data formatting | bytes 37748736
  511.6 0.0 slice-done
  511.6 0.0 slice-done.1
  511.6 0.0 slice-done.2
  511.6 6.9 %copy.10 = bf16[3072,3072]{1,0:T(8,128)(2,1)} copy(bf16[3072,3072]{1,0:T(8,128)(2,1)S(1)} %bitcast.10) | data formatting | bytes 37748736
  (11 shorter events, 0.0 us)
Async XLA Ops:
  7.2 289.9 %all-gather.3.cloned.1.call-start = ((), (), s32[]{:S(2)}) async-start(), calls=%async_computation.3 | async-start | bytes 23592960 | tf_op jit(solution)/shard_map/all_gather | solution.py:22
  178.9 240.2 %all-gather.5.cloned.1.call-start = ((), (), s32[]{:S(2)}) async-start(), calls=%async_computation.4 | async-start | bytes 23592960 | tf_op jit(solution)/shard_map/all_gather | solution.py:23
  185.7 1.8 copy-start
  185.7 304.7 %reduce-scatter.2.cloned.1.call-start = ((), (), s32[]{:S(2)}) async-start(), calls=%async_computation.5 | async-start | bytes 3932160 | tf_op jit(solution)/shard_map/reduce_scatter | solution.py:30
  490.4 21.2 %slice-start = ((s8[18874368]{0:T(1024)(128)(4,1)}), s8[4194304]{0:T(1024)(128)(4,1)S(1)}, s32[]{:S(2)}) async-start(s8[18874368]{0:T(1024)(128)(4,1)} %bitcast.9), calls=%async_computation.6 | async-start | bytes 8388608
  492.5 19.1 %slice-start.1 = ((s8[18874368]{0:T(1024)(128)(4,1)}), s8[4194304]{0:T(1024)(128)(4,1)S(1)}, s32[]{:S(2)}) async-start(s8[18874368]{0:T(1024)(128)(4,1)} %bitcast.9), calls=%async_computation.7 | async-start | bytes 8388608
  492.5 19.1 %slice-start.2 = ((s8[18874368]{0:T(1024)(128)(4,1)}), s8[4194304]{0:T(1024)(128)(4,1)S(1)}, s32[]{:S(2)}) async-start(s8[18874368]{0:T(1024)(128)(4,1)} %bitcast.9), calls=%async_computation.8 | async-start | bytes 8388608
  492.5 19.1 %slice-start.3 = ((s8[18874368]{0:T(1024)(128)(4,1)}), s8[4194304]{0:T(1024)(128)(4,1)S(1)}, s32[]{:S(2)}) async-start(s8[18874368]{0:T(1024)(128)(4,1)} %bitcast.9), calls=%async_computation.9 | async-start | bytes 8388608
  492.5 19.1 %slice-start.4 = ((s8[18874368]{0:T(1024)(128)(4,1)}), s8[2097152]{0:T(1024)(128)(4,1)S(1)}, s32[]{:S(2)}) async-start(s8[18874368]{0:T(1024)(128)(4,1)} %bitcast.9), calls=%async_computation.10 | async-start | bytes 4194304
Sparse Core Ops, SparseCore 0:
  179.1 117.9 all-gather.2
  299.2 119.9 all-gather.4
  430.0 60.3 reduce-scatter.1
where the time goes:
time: 525 us
  waiting for transfers between devices  282 us (54%)
  blocking collectives  167 us (32%)
  local copies, waits for them, and re-layouts  27.7 us (5%)
  matrix products  20.1 us (4%)
  other arithmetic  14.7 us (3%)
  between operations  13.8 us (3%)
    all_gather x1, waiting for transfers between devices, shards(): lax.all_gather(down_cast, 'tp', axis=1, tiled=True)  113 us
    all_to_all x1, blocking collectives, shards(): lax.all_to_all(quarter, 'fs', split_axis=1, concat_axis=0, tiled=True)  109 us
    all_gather x1, waiting for transfers between devices, shards(): lax.all_gather(stacked, 'tp', axis=1, tiled=True)  109 us
    reduce_scatter x1, waiting for transfers between devices, shards(): summed = lax.psum_scatter(terms, 'fs', scatter_dimension=1, tiled=True)  60.6 us
    all_to_all x1, blocking collectives, shards(): lax.all_to_all(up_cast, 'tp', split_axis=0, concat_axis=1, tiled=True)  57.8 us
    unnamed x14, local copies, waits for them, and re-layouts  27.7 us
    dot_general x1, matrix products, shards(): terms = jnp.dot(hidden, sampled_down, preferred_element_type=jnp.float32)  10.7 us
  transfers between devices with their start and end apart: 3, of which 3 were waited for; matrix products, arithmetic and copies ran while one was open for 3% of the time, Pallas kernels for 0%

commit v1 on v0

--- a/solution.py
+++ b/solution.py
@@ -2,6 +2,7 @@
 import jax.numpy as jnp
 from jax import lax
 from jax.sharding import PartitionSpec as P
+from jax.lax import all_gather
 
 
 def normalize(tokens):
@@ -19,7 +20,7 @@
     part_rows = quarter.shape[0]
     stacked = moved.reshape(moved.shape[0] // part_rows, part_rows, moved.shape[1])
     joined, sampled_down = (
-        lax.all_gather(stacked, "tp", axis=1, tiled=True),
+        jnp.concatenate(all_gather(stacked, "tp"), axis=1),
         lax.all_gather(down_cast, "tp", axis=1, tiled=True),
     )
     sampled_up = joined.reshape(joined.shape[0] * joined.shape[1], joined.shape[2])

time: 525 us -> 517 us (0.985)
  waiting for transfers between devices: 282 us -> 266 us
  local copies, waits for them, and re-layouts: 27.7 us -> 38.9 us
    all_gather x1, waiting for transfers between devices: 113 us -> 96.1 us  [shards(): lax.all_gather(down_cast, 'tp', axis=1, tiled=True)]
    reshape x0 -> x1, local copies, waits for them, and re-layouts: none -> 10.1 us  [shards(): jnp.concatenate(all_gather(stacked, 'tp'), axis=1)]
    unnamed x14 -> x5, local copies, waits for them, and re-layouts: 27.7 us -> 28.9 us
  transfers between devices with their start and end apart: 3 -> 3, of which waited for: 3 -> 3; matrix products, arithmetic and copies ran while one was open for 3% -> 4% of each run, Pallas kernels for 0% -> 0%
where the time goes in v1:
time: 517 us; the launch traced here: 516 us
  waiting for transfers between devices  266 us (51%)
  blocking collectives  167 us (32%)
  local copies, waits for them, and re-layouts  38.9 us (8%)
  matrix products  16 us (3%)
  other arithmetic  14.5 us (3%)
  between operations  13.8 us (3%)
    all_gather x1, waiting for transfers between devices, shards(): all_gather(stacked, 'tp')  110 us
    all_to_all x1, blocking collectives, shards(): lax.all_to_all(quarter, 'fs', split_axis=1, concat_axis=0, tiled=True)  109 us
    all_gather x1, waiting for transfers between devices, shards(): lax.all_gather(down_cast, 'tp', axis=1, tiled=True)  96.1 us
    reduce_scatter x1, waiting for transfers between devices, shards(): summed = lax.psum_scatter(terms, 'fs', scatter_dimension=1, tiled=True)  60.6 us
    all_to_all x1, blocking collectives, shards(): lax.all_to_all(up_cast, 'tp', split_axis=0, concat_axis=1, tiled=True)  57.8 us
    unnamed x5, local copies, waits for them, and re-layouts  28.9 us
    dot_general x1, matrix products, shards(): terms = jnp.dot(hidden, sampled_down, preferred_element_type=jnp.float32)  10.7 us
  transfers between devices with their start and end apart: 3, of which 3 were waited for; matrix products, arithmetic and copies ran while one was open for 4% of the time, Pallas kernels for 0%

profile of v1, /device:TPU:0, one launch (start us, length us, event | category | flops | bytes accessed | tf_op | source)
XLA Modules:
  0.0 516.2 jit_solution(2515850050477024355)
XLA Ops:
  7.2 0.0 all-gather.6.cloned.1.call-start
  7.2 5.1 multiply_convert_fusion
  12.3 57.8 %all_to_all.29 = bf16[4,192,3072]{2,1,0:T(8,128)(2,1)S(1)} all-to-all(bf16[4,192,3072]{2,1,0:T(8,128)(2,1)S(1)} %bitcast.15), channel_id=1, replica_groups=mesh['grp'=2,'fs'=4,'tp'=4] {'tp'}, dimensions={0} | all-to-all | bytes 9437184 | tf_op jit(solution)/shard_map/all_to_all | solution.py:18
  70.1 108.8 %all_to_all.30 = bf16[192,4,3072]{2,0,1:T(8,128)(2,1)} all-to-all(bf16[192,4,3072]{2,0,1:T(8,128)(2,1)S(1)} %bitcast.14), channel_id=1, replica_groups=mesh['grp'=2,'fs'=4,'tp'=4] {'fs'}, dimensions={1} | all-to-all | bytes 9437184 | tf_op jit(solution)/shard_map/all_to_all | solution.py:19
  178.9 0.0 all-gather.6.cloned.1.call-update
  178.9 0.0 all-gather.4.cloned.1.call-start
  179.0 6.6 %convert_element_type.22 = bf16[3072,768]{1,0:T(8,128)(2,1)} convert(f32[3072,768]{1,0:T(8,128)} %param.6) | non-fusion elementwise | flops 2359296 | bytes 14155776 | tf_op jit(solution)/shard_map/convert_element_type | solution.py:17
  185.6 0.0 copy-start.1
  185.6 0.0 all-gather.4.cloned.1.call-update
  185.6 0.0 reduce-scatter.2.cloned.1.call-start
  185.7 1.7 copy-done.1
  187.3 0.3 convert_reduce_fusion
  187.6 0.6 fusion.4
  188.2 109.6 %all-gather.6.cloned.1.call-done = bf16[16,192,3072]{2,1,0:T(8,128)(2,1)} async-done(((bf16[4,192,3072]{2,1,0:T(8,128)(2,1)}), bf16[16,192,3072]{2,1,0:T(8,128)(2,1)}) %all-gather.6.cloned.1.call-update) | async-done | bytes 18874384 | tf_op jit(solution)/shard_map/all_gather | solution.py:23
  297.8 10.1 %copy.8 = bf16[4,4,192,3072]{3,2,1,0:T(8,128)(2,1)S(1)} copy(bf16[4,4,192,3072]{3,2,0,1:T(8,128)(2,1)} %bitcast.12) | data formatting | bytes 37748736 | tf_op jit(solution)/shard_map/reshape | solution.py:23
  307.9 0.0 copy-start
  307.9 10.6 %copy-done = bf16[4,4,192,3072]{3,2,1,0:T(8,128)(2,1)} copy-done((bf16[4,4,192,3072]{3,2,1,0:T(8,128)(2,1)}, bf16[4,4,192,3072]{3,2,1,0:T(8,128)(2,1)S(1)}, u32[]{:S(2)}) %copy-start) | copy-done | bytes 18874392
  318.5 5.3 %fusion.1 = bf16[256,3072]{1,0:T(8,128)(2,1)S(1)} fusion(bf16[3072,3072]{1,0:T(8,128)(2,1)S(1)} %bitcast.10, bf16[256,3072]{1,0:T(8,128)(2,1)S(1)} %copy-done.1, f32[256]{0:T(256)S(1)} %add_rsqrt_fusion, f32[256]{0:T(256)S(1)} %broadcast_multiply_fusion), kind=kOutput, calls=%fused_computation.5 | convolution fusion | flops 4837343232 | bytes 22022144 | tf_op jit(solution)/shard_map/dot_general | solution.py:28
  323.8 96.1 %all-gather.4.cloned.1.call-done = bf16[3072,3072]{1,0:T(8,128)(2,1)} async-done(((bf16[3072,768]{1,0:T(8,128)(2,1)}), bf16[3072,3072]{1,0:T(8,128)(2,1)}) %all-gather.4.cloned.1.call-update) | async-done | bytes 18874384 | tf_op jit(solution)/shard_map/all_gather | solution.py:24
  420.0 10.7 %fusion.9 = f32[256,3072]{1,0:T(8,128)} fusion(bf16[256,3072]{1,0:T(8,128)(2,1)S(1)} %fusion.1, bf16[3072,3072]{1,0:T(8,128)(2,1)} %all-gather.4.cloned.1.call-done), kind=kOutput, calls=%fused_computation.14 | convolution fusion | flops 4831838208 | bytes 23592960 | tf_op jit(solution)/shard_map/dot_general | solution.py:30
  430.6 0.0 reduce-scatter.2.cloned.1.call-update
  430.6 60.6 %reduce-scatter.2.cloned.1.call-done = f32[256,768]{1,0:T(8,128)} async-done(((f32[256,3072]{1,0:T(8,128)}), f32[256,768]{1,0:T(8,128)}) %reduce-scatter.2.cloned.1.call-update) | async-done | bytes 786448 | tf_op jit(solution)/shard_map/reduce_scatter | solution.py:31
  491.2 1.9 convert_element_type.23
  493.1 16.6 %copy.10 = bf16[3072,3072]{1,0:T(8,128)(2,1)} copy(bf16[3072,3072]{1,0:T(8,128)(2,1)} %all-gather.4.cloned.1.call-done) | data formatting | bytes 37748736
  (2 shorter events, 0.0 us)
Async XLA Ops:
  7.2 290.6 %all-gather.6.cloned.1.call-start = ((), (), s32[]{:S(2)}) async-start(), calls=%async_computation.5 | async-start | bytes 23592960 | tf_op jit(solution)/shard_map/all_gather | solution.py:23
  178.9 241.0 %all-gather.4.cloned.1.call-start = ((), (), s32[]{:S(2)}) async-start(), calls=%async_computation.3 | async-start | bytes 23592960 | tf_op jit(solution)/shard_map/all_gather | solution.py:24
  185.6 1.7 copy-start.1
  185.6 305.6 %reduce-scatter.2.cloned.1.call-start = ((), (), s32[]{:S(2)}) async-start(), calls=%async_computation.4 | async-start | bytes 3932160 | tf_op jit(solution)/shard_map/reduce_scatter | solution.py:31
  307.9 10.6 %copy-start = (bf16[4,4,192,3072]{3,2,1,0:T(8,128)(2,1)}, bf16[4,4,192,3072]{3,2,1,0:T(8,128)(2,1)S(1)}, u32[]{:S(2)}) copy-start(bf16[4,4,192,3072]{3,2,1,0:T(8,128)(2,1)S(1)} %copy.8) | copy-start | bytes 56623108
Sparse Core Ops, SparseCore 0:
  179.1 118.6 all-gather.5
  299.9 119.9 all-gather.3
  430.8 60.3 reduce-scatter.1
